TPU v7x, 32 devices: a whole 2x2x4 slice. The times are simulated.
32 devices in a mesh: gr: 2 (over x), fs: 8 (over z, y), tp: 2 (over core).
Axes of the slice: x: 2, y: 2, z: 4, core: 2. Of those that a mesh axis runs over, the one named last changes fastest.
Arguments:
- tokens: bfloat16 [4096, 2048], P(('gr', 'fs', 'tp')), may hold values from -6 to 6
- routes: int32 [4096, 8], P(('gr', 'fs', 'tp')), may hold values from 0 to 15, all different within a row; in each aligned block of 128 rows (0 to 127, 128 to 255, ...) at most 96 rows name the same one
- route_weights: float32 [4096, 8], P(('gr', 'fs', 'tp')), may hold values from 0.1 to 0.6
- norm_gain: float32 [2048], P(('gr', 'tp')), may hold values from 0.1 to 1.9
- gate_trained: float32 [16, 384, 2048], P(None, 'fs', ('gr', 'tp')), may hold values from -0.125 to 0.125
- up_trained: float32 [16, 384, 2048], P(None, 'fs', ('gr', 'tp')), may hold values from -0.125 to 0.125
- down_trained: float32 [16, 384, 2048], P(None, 'fs', ('gr', 'tp')), may hold values from -0.3125 to 0.3125
- shared_gate_trained: float32 [512, 2048], P('fs', ('gr', 'tp')), may hold values from -0.125 to 0.125
- shared_up_trained: float32 [512, 2048], P('fs', ('gr', 'tp')), may hold values from -0.125 to 0.125
- shared_down_trained: float32 [512, 2048], P('fs', ('gr', 'tp')), may hold values from -0.25 to 0.25
Outputs:
- combined: bfloat16 [4096, 2048], P(('gr', 'fs', 'tp'))
- expert_gate: bfloat16 [16, 384, 2048], P(('fs', 'tp'))
- expert_up: bfloat16 [16, 384, 2048], P(('fs', 'tp'))
- expert_down: bfloat16 [16, 384, 2048], P(('fs', 'tp'))
- shared_gate: bfloat16 [512, 2048], P('fs')
- shared_up: bfloat16 [512, 2048], P('fs')
- shared_down: bfloat16 [512, 2048], P('fs')
Inputs may be any that keep to these rules, and one draw needn't show every extreme that they name: `routes`: each row names 8 different experts. Among the rows of one device no expert is named more than 96 times, and that many is reached in every draw.
All inputs are finite; a program needn't handle non-finite values.
Results may differ from a plain program's by a relative error of at most 0.0084.
Values may be sent and summed in bfloat16 or wider, within the bound.
A program may use at most 128 MiB of HBM per device.

v0:
```python
import jax
import jax.numpy as jnp
from jax import lax
from jax.sharding import PartitionSpec as P

epsilon = 1e-06


def contract_rows(inputs, matrix):
    return lax.dot_general(
        inputs, matrix, (((1,), (1,)), ((), ())), preferred_element_type=jnp.float32
    )


def swiglu_rows(inputs, gate_matrix, up_matrix, down_matrix):
    hidden = (
        jax.nn.silu(contract_rows(inputs, gate_matrix)) * contract_rows(inputs, up_matrix)
    ).astype(jnp.bfloat16)
    return jnp.dot(hidden, down_matrix, preferred_element_type=jnp.float32)


def body(
    tokens,
    routes,
    route_weights,
    norm_gain,
    gate_trained,
    up_trained,
    down_trained,
    shared_gate_trained,
    shared_up_trained,
    shared_down_trained,
):
    gain_row = norm_gain[None, None, :]
    stacked = jnp.stack(
        [gate_trained * gain_row, up_trained * gain_row, down_trained], axis=1
    ).astype(jnp.bfloat16)
    halves = lax.all_to_all(
        lax.all_to_all(stacked[:, :, :, None, :], "fs", split_axis=0, concat_axis=2, tiled=True),
        "tp",
        split_axis=0,
        concat_axis=3,
        tiled=True,
    )
    owned = lax.all_gather(halves[:, :, :, None], "gr", axis=3, tiled=True)
    owned = owned.reshape(owned.shape[0], 3, owned.shape[2], -1)
    expert_gate = owned[:, 0]
    expert_up = owned[:, 1]
    expert_down = owned[:, 2]
    shared_gain = norm_gain[None, :]
    shared_stack = jnp.stack(
        [shared_gate_trained * shared_gain, shared_up_trained * shared_gain, shared_down_trained],
        axis=0,
    ).astype(jnp.bfloat16)
    shared_whole = lax.all_gather(shared_stack, ("gr", "tp"), axis=2, tiled=True)
    shared_gate = shared_whole[0]
    shared_up = shared_whole[1]
    shared_down = shared_whole[2]
    values = tokens.astype(jnp.float32)
    normed = (
        values * lax.rsqrt(jnp.mean(values * values, axis=1, keepdims=True) + epsilon)
    ).astype(jnp.bfloat16)
    row_count, features = normed.shape
    per_token = routes.shape[1]
    shared_out = swiglu_rows(
        normed,
        lax.all_gather(shared_gate, "fs", axis=0, tiled=True),
        lax.all_gather(shared_up, "fs", axis=0, tiled=True),
        lax.all_gather(shared_down, "fs", axis=0, tiled=True),
    )
    experts = lax.axis_size("fs") * lax.axis_size("tp")
    capacity = max(2, 3 * row_count * per_token // (2 * experts))
    chosen = routes.reshape(-1)
    onehot = (chosen[:, None] == jnp.arange(experts, dtype=jnp.int32)[None, :]).astype(jnp.int32)
    position = jnp.sum((jnp.cumsum(onehot, axis=0) - onehot) * onehot, axis=1)
    target = chosen * capacity + position
    source = (
        jnp.full((experts * capacity,), row_count, jnp.int32)
        .at[target]
        .set(jnp.arange(row_count * per_token, dtype=jnp.int32) // per_token)
    )
    padded = jnp.concatenate([normed, jnp.zeros((1, features), jnp.bfloat16)], axis=0)
    outgoing = padded[source].reshape(experts, capacity, features)
    arrived = lax.all_to_all(outgoing, ("fs", "tp"), split_axis=0, concat_axis=0, tiled=True)
    item_count = arrived.shape[1]
    result = swiglu_rows(
        arrived.reshape(-1, features), expert_gate[0], expert_up[0], expert_down[0]
    )
    result = result.astype(jnp.bfloat16).reshape(experts, item_count, features)
    returned = lax.all_to_all(result, ("fs", "tp"), split_axis=0, concat_axis=0, tiled=True)
    picked = returned.reshape(experts * capacity, features)[target].astype(jnp.float32)
    picked = picked.reshape(row_count, per_token, features)
    routed = jnp.sum(picked * route_weights[:, :, None], axis=1)
    combined = (routed + shared_out).astype(jnp.bfloat16)
    return (combined, expert_gate, expert_up, expert_down, shared_gate, shared_up, shared_down)


def solution(mesh):
    in_specs = (
        P(("gr", "fs", "tp"), None),
        P(("gr", "fs", "tp"), None),
        P(("gr", "fs", "tp"), None),
        P(("gr", "tp")),
        P(None, "fs", ("gr", "tp")),
        P(None, "fs", ("gr", "tp")),
        P(None, "fs", ("gr", "tp")),
        P("fs", ("gr", "tp")),
        P("fs", ("gr", "tp")),
        P("fs", ("gr", "tp")),
    )
    out_specs = (
        P(("gr", "fs", "tp"), None),
        P(("fs", "tp"), None, None),
        P(("fs", "tp"), None, None),
        P(("fs", "tp"), None, None),
        P("fs", None),
        P("fs", None),
        P("fs", None),
    )
    return jax.shard_map(body, mesh=mesh, in_specs=in_specs, out_specs=out_specs, check_vma=False)
```

profile of v0, /device:TPU:0, one launch (start us, length us, event | category | flops | bytes accessed | tf_op | source)
XLA Modules:
  0.0 506.6 jit_solution(6187070013755928364)
XLA Ops:
  13.5 7.4 %all-to-all-start.1 = ((bf16[16,3,48,1,512]{4,2,3,1,0:T(8,128)(2,1)}), bf16[16,3,48,1,512]{4,2,3,1,0:T(8,128)(2,1)S(1)}, u32[]{:S(2)}, u32[]{:S(2)}) async-start(bf16[16,3,48,1,512]{4,2,3,1,0:T(8,128)(2,1)} %pad_maximum_fusion), calls=%async_computation.1 | async-start | bytes 4718592 | tf_op jit(solution)/shard_map/all_to_all | solution.py:39
  21.2 4.5 reduce-window.6
  26.9 4.3 scatter_custom_fusion
  31.2 7.1 %gather_fusion = bf16[1536,2048]{1,0:T(8,128)(2,1)} fusion(bf16[129,2048]{1,0:T(8,128)(2,1)S(1)} %concatenate.11, s32[2048]{0:T(1024)S(1)} %pad_clamp_fusion), kind=kCustom, calls=%fused_computation | custom fusion | bytes 12589056 | tf_op jit(solution)/shard_map/gather | solution.py:83
  38.3 36.5 %all-to-all-done.1 = bf16[16,3,48,1,512]{4,2,3,1,0:T(8,128)(2,1)S(1)} async-done(((bf16[16,3,48,1,512]{4,2,3,1,0:T(8,128)(2,1)}), bf16[16,3,48,1,512]{4,2,3,1,0:T(8,128)(2,1)S(1)}, u32[]{:S(2)}, u32[]{:S(2)}) %all-to-all-start.1) | async-done | bytes 2359328 | tf_op jit(solution)/shard_map/all_to_all | solution.py:39
  74.9 6.5 %all_to_all.43 = bf16[2,3,384,1,512]{4,2,1,3,0:T(8,128)(2,1)} all-to-all(bf16[2,3,384,1,512]{4,2,1,3,0:T(8,128)(2,1)S(1)} %bitcast.99), channel_id=1, replica_groups=mesh['gr'=2,'fs'=8,'tp'=2] {'tp'}, dimensions={0} | all-to-all | bytes 4718592 | tf_op jit(solution)/shard_map/all_to_all | solution.py:38
  81.5 4.7 all-to-all-start
  86.9 65.5 %all-gather.9.cloned.1.call-done = bf16[1,3,384,4,1,512]{5,2,4,1,0,3:T(8,128)(2,1)} async-done(((bf16[1,3,384,2,1,512]{5,2,4,1,0,3:T(8,128)(2,1)}), bf16[1,3,384,4,1,512]{5,2,4,1,0,3:T(8,128)(2,1)}) %all-gather.9.cloned.1.call-update) | async-done | bytes 4718608 | tf_op jit(solution)/shard_map/all_gather | solution.py:45
  152.4 6.6 %copy.45 = bf16[1,3,384,4,1,512]{2,5,3,1,4,0:T(8,128)(2,1)} copy(bf16[1,3,384,4,1,512]{5,2,4,1,0,3:T(8,128)(2,1)} %all-gather.9.cloned.1.call-done) | data formatting | bytes 9437184 | tf_op jit(solution)/shard_map/all_gather | solution.py:45
  159.0 41.1 %all-to-all-done = bf16[16,96,2048]{2,1,0:T(8,128)(2,1)} async-done(((bf16[16,96,2048]{2,1,0:T(8,128)(2,1)}), bf16[16,96,2048]{2,1,0:T(8,128)(2,1)}, u32[]{:S(2)}, u32[]{:S(2)}) %all-to-all-start) | async-done | bytes 6291488 | tf_op jit(solution)/shard_map/all_to_all | solution.py:84
  200.2 5.9 %fusion.10 = f32[1536,384]{1,0:T(8,128)S(1)} fusion(bf16[1536,2048]{1,0:T(8,128)(2,1)} %bitcast.5, bf16[1,3,384,2048]{2,3,1,0:T(8,128)(2,1)} %bitcast.94), kind=kOutput, calls=%fused_computation.18 | convolution fusion | flops 2415919104 | bytes 10223616 | tf_op jit(solution)/shard_map/dot_general | solution.py:10
  206.1 11.4 %convolution_convert_fusion = bf16[1536,2048]{1,0:T(8,128)(2,1)} fusion(bf16[1,3,384,2048]{2,3,1,0:T(8,128)(2,1)} %bitcast.95, bf16[1536,2048]{1,0:T(8,128)(2,1)} %bitcast.5, f32[1536,384]{1,0:T(8,128)S(1)} %fusion.10), kind=kOutput, calls=%fused_computation.5 | convolution fusion | flops 4838522880 | bytes 18087936 | tf_op jit(solution)/shard_map/dot_general | solution.py:19
  217.5 28.2 %all-to-all-start.3 = ((bf16[16,96,2048]{2,1,0:T(8,128)(2,1)}), bf16[16,96,2048]{2,1,0:T(8,128)(2,1)}, u32[]{:S(2)}, u32[]{:S(2)}) async-start(bf16[16,96,2048]{2,1,0:T(8,128)(2,1)} %bitcast.100), calls=%async_computation.3 | async-start | bytes 12582912 | tf_op jit(solution)/shard_map/all_to_all | solution.py:90
  245.9 8.7 %all_gather.16 = bf16[3,64,2048]{2,1,0:T(8,128)(2,1)S(1)} all-gather(bf16[3,64,512]{2,1,0:T(8,128)(2,1)S(1)} %pad_maximum_fusion.1), channel_id=1, replica_groups=mesh['gr'=2,'fs'=8,'tp'=2] {'gr','tp'}, dimensions={2}, use_global_device_ids=true | all-gather | bytes 983040 | tf_op jit(solution)/shard_map/all_gather | solution.py:55
  257.1 111.5 %all-gather.11.cloned.1.call-done = bf16[1,512,2048]{2,1,0:T(8,128)(2,1)} async-done(((bf16[1,64,2048]{2,1,0:T(8,128)(2,1)}), bf16[1,512,2048]{2,1,0:T(8,128)(2,1)}) %all-gather.11.cloned.1.call-update) | async-done | bytes 2097168 | tf_op jit(solution)/shard_map/all_gather | solution.py:67
  371.0 4.5 slice_bitcast_fusion
  375.5 2.6 copy.47
  378.1 2.6 copy.48
  382.3 2.8 all-to-all-done.3
  385.1 12.4 %gather_fusion.1 = bf16[1024,2048]{1,0:T(8,128)(2,1)} fusion(bf16[1536,2048]{1,0:T(8,128)(2,1)} %bitcast.21, s32[1024]{0:T(1024)S(1)} %broadcast_clamp_fusion), kind=kCustom, calls=%fused_computation.1 | custom fusion | bytes 8392704 | tf_op jit(solution)/shard_map/gather | solution.py:91
  397.5 6.5 %fusion = f32[128,2048]{1,0:T(8,128)S(1)} fusion(bf16[1024,2048]{1,0:T(8,128)(2,1)} %gather_fusion.1, f32[128,8]{1,0:T(8,128)S(1)} %copy.46), kind=kLoop, calls=%fused_computation.4 | loop fusion | flops 6029312 | bytes 5246976 | tf_op jit(solution)/shard_map/reduce_sum | solution.py:93
  404.0 40.6 %all-gather.13.cloned.1.call-done = bf16[1,512,2048]{2,1,0:T(8,128)(2,1)} async-done(((bf16[1,64,2048]{2,1,0:T(8,128)(2,1)}), bf16[1,512,2048]{2,1,0:T(8,128)(2,1)}) %all-gather.13.cloned.1.call-update) | async-done | bytes 2097168 | tf_op jit(solution)/shard_map/all_gather | solution.py:68
  444.6 50.2 %all-gather.15.cloned.1.call-done = bf16[1,512,2048]{2,1,0:T(8,128)(2,1)} async-done(((bf16[1,64,2048]{2,1,0:T(8,128)(2,1)}), bf16[1,512,2048]{2,1,0:T(8,128)(2,1)}) %all-gather.15.cloned.1.call-update) | async-done | bytes 2097168 | tf_op jit(solution)/shard_map/all_gather | solution.py:69
  494.7 4.3 fusion.2
  (58 shorter events, 14.3 us)
Async XLA Ops:
  8.0 1.7 copy-start.6
  8.0 1.9 copy-start.1
  13.5 7.4 %copy-start.5 = (s32[128,8]{0,1:T(8,128)S(1)}, s32[128,8]{0,1:T(8,128)}, u32[]{:S(2)}) copy-start(s32[128,8]{0,1:T(8,128)} %param.11) | copy-start | bytes 12292
  13.5 12.8 %copy-start = (bf16[128,2048]{1,0:T(8,128)(2,1)S(1)}, bf16[128,2048]{1,0:T(8,128)(2,1)}, u32[]{:S(2)}) copy-start(bf16[128,2048]{1,0:T(8,128)(2,1)} %param.10) | copy-start | bytes 1572868
  13.5 61.3 %all-to-all-start.1 = ((bf16[16,3,48,1,512]{4,2,3,1,0:T(8,128)(2,1)}), bf16[16,3,48,1,512]{4,2,3,1,0:T(8,128)(2,1)S(1)}, u32[]{:S(2)}, u32[]{:S(2)}) async-start(bf16[16,3,48,1,512]{4,2,3,1,0:T(8,128)(2,1)} %pad_maximum_fusion), calls=%async_computation.1 | async-start | bytes 4718592 | tf_op jit(solution)/shard_map/all_to_all | solution.py:39
  81.5 118.7 %all-to-all-start = ((bf16[16,96,2048]{2,1,0:T(8,128)(2,1)}), bf16[16,96,2048]{2,1,0:T(8,128)(2,1)}, u32[]{:S(2)}, u32[]{:S(2)}) async-start(bf16[16,96,2048]{2,1,0:T(8,128)(2,1)} %bitcast.93), calls=%async_computation | async-start | bytes 12582912 | tf_op jit(solution)/shard_map/all_to_all | solution.py:84
  86.2 66.2 %all-gather.9.cloned.1.call-start = ((), (), s32[]{:S(2)}) async-start(), calls=%async_computation.4 | async-start | bytes 7077888 | tf_op jit(solution)/shard_map/all_gather | solution.py:45
  217.5 28.3 %copy-start.4 = (f32[64,512]{1,0:T(8,128)S(1)}, f32[64,512]{1,0:T(8,128)}, u32[]{:S(2)}) copy-start(f32[64,512]{1,0:T(8,128)} %param.19) | copy-start | bytes 393220
  217.5 28.3 %copy-start.2 = (f32[64,512]{1,0:T(8,128)S(1)}, f32[64,512]{1,0:T(8,128)}, u32[]{:S(2)}) copy-start(f32[64,512]{1,0:T(8,128)} %param.17) | copy-start | bytes 393220
  217.5 28.3 %copy-start.3 = (f32[64,512]{1,0:T(8,128)S(1)}, f32[64,512]{1,0:T(8,128)}, u32[]{:S(2)}) copy-start(f32[64,512]{1,0:T(8,128)} %param.18) | copy-start | bytes 393220
  217.5 167.6 %all-to-all-start.3 = ((bf16[16,96,2048]{2,1,0:T(8,128)(2,1)}), bf16[16,96,2048]{2,1,0:T(8,128)(2,1)}, u32[]{:S(2)}, u32[]{:S(2)}) async-start(bf16[16,96,2048]{2,1,0:T(8,128)(2,1)} %bitcast.100), calls=%async_computation.3 | async-start | bytes 12582912 | tf_op jit(solution)/shard_map/all_to_all | solution.py:90
  245.7 122.9 %all-gather.11.cloned.1.call-start = ((), (), s32[]{:S(2)}) async-start(), calls=%async_computation.5 | async-start | bytes 2359296 | tf_op jit(solution)/shard_map/all_gather | solution.py:67
  245.9 11.2 %copy-start.7 = (f32[128,8]{0,1:T(8,128)S(1)}, f32[128,8]{0,1:T(8,128)}, u32[]{:S(2)}) copy-start(f32[128,8]{0,1:T(8,128)} %param.12) | copy-start | bytes 12292
  255.8 188.7 %all-gather.13.cloned.1.call-start = ((), (), s32[]{:S(2)}) async-start(), calls=%async_computation.6 | async-start | bytes 2359296 | tf_op jit(solution)/shard_map/all_gather | solution.py:68
  256.4 238.3 %all-gather.15.cloned.1.call-start = ((), (), s32[]{:S(2)}) async-start(), calls=%async_computation.7 | async-start | bytes 2359296 | tf_op jit(solution)/shard_map/all_gather | solution.py:69
Sparse Core Ops, SparseCore 0:
  88.5 63.8 all-gather.8
Sparse Core Ops, SparseCore 1:
  255.9 112.6 all-gather.10
  370.6 73.9 all-gather.12
  447.1 47.5 all-gather.14
where the time goes:
time: 507 us
  waiting for transfers between devices  350 us (69%)
  local copies, waits for them, and re-layouts  44.2 us (9%)
  starting transfers between devices  40.7 us (8%)
  matrix products  24 us (5%)
  other arithmetic  16.8 us (3%)
  between operations  15.9 us (3%)
  blocking collectives  15.2 us (3%)
    all_gather x1, waiting for transfers between devices, body(): lax.all_gather(shared_gate, 'fs', axis=0, tiled=True)  111 us
    all_gather x1, waiting for transfers between devices, body(): owned = lax.all_gather(halves[:, :, :, None], 'gr', axis=3, tiled=True)  65.5 us
    all_gather x1, waiting for transfers between devices, body(): lax.all_gather(shared_down, 'fs', axis=0, tiled=True)  50.2 us
    all_to_all x1, waiting for transfers between devices, body(): lax.all_to_all(outgoing, ('fs', 'tp'), split_axis=0, concat_axis=0, tiled...  41.1 us
    all_gather x1, waiting for transfers between devices, body(): lax.all_gather(shared_up, 'fs', axis=0, tiled=True)  40.6 us
    all_to_all x1, waiting for transfers between devices, body(): lax.all_to_all(stacked[:, :, :, None, :], 'fs', split_axis=0, concat_axis...  36.5 us
    all_to_all x1, starting transfers between devices, body(): lax.all_to_all(result, ('fs', 'tp'), split_axis=0, concat_axis=0, tiled=T...  28.2 us
    dot_general x2, matrix products, swiglu_rows(): return jnp.dot(hidden, down_matrix, preferred_element_type=jnp.float32)  15.6 us
  transfers between devices with their start and end apart: 7, of which 7 were waited for; matrix products, arithmetic and copies ran while one was open for 11% of the time, Pallas kernels for 0%

commit v1 on v0

--- a/solution.py
+++ b/solution.py
@@ -35,12 +35,22 @@
     stacked = jnp.stack(
         [gate_trained * gain_row, up_trained * gain_row, down_trained], axis=1
     ).astype(jnp.bfloat16)
-    halves = lax.all_to_all(
-        lax.all_to_all(stacked[:, :, :, None, :], "fs", split_axis=0, concat_axis=2, tiled=True),
-        "tp",
-        split_axis=0,
-        concat_axis=3,
-        tiled=True,
+    halves = jnp.concatenate(
+        lax.all_to_all(
+            jnp.stack(
+                jnp.split(
+                    lax.all_to_all(
+                        stacked[:, :, :, None, :], "fs", split_axis=0, concat_axis=2, tiled=True
+                    ),
+                    lax.axis_size("tp"),
+                    axis=0,
+                )
+            ),
+            "tp",
+            0,
+            0,
+        ),
+        axis=3,
     )
     owned = lax.all_gather(halves[:, :, :, None], "gr", axis=3, tiled=True)
     owned = owned.reshape(owned.shape[0], 3, owned.shape[2], -1)

time: 507 us -> 508 us (level)
  no operation moved by 1% of the time
where the time goes in v1:
time: 508 us; the launch traced here: 507 us
  waiting for transfers between devices  350 us (69%)
  local copies, waits for them, and re-layouts  44.4 us (9%)
  starting transfers between devices  40.7 us (8%)
  matrix products  24 us (5%)
  other arithmetic  17 us (3%)
  between operations  15.9 us (3%)
  blocking collectives  15.3 us (3%)
    all_gather x1, waiting for transfers between devices, body(): lax.all_gather(shared_gate, 'fs', axis=0, tiled=True)  111 us
    all_gather x1, waiting for transfers between devices, body(): owned = lax.all_gather(halves[:, :, :, None], 'gr', axis=3, tiled=True)  65.5 us
    all_gather x1, waiting for transfers between devices, body(): lax.all_gather(shared_down, 'fs', axis=0, tiled=True)  50.2 us
    all_to_all x1, waiting for transfers between devices, body(): lax.all_to_all(outgoing, ('fs', 'tp'), split_axis=0, concat_axis=0, tiled...  41.1 us
    all_gather x1, waiting for transfers between devices, body(): lax.all_gather(shared_up, 'fs', axis=0, tiled=True)  40.6 us
    all_to_all x1, waiting for transfers between devices, body(): lax.all_to_all(stacked[:, :, :, None, :], 'fs', split_axis=0, concat_axis...  36.5 us
    all_to_all x1, starting transfers between devices, body(): lax.all_to_all(result, ('fs', 'tp'), split_axis=0, concat_axis=0, tiled=T...  28.2 us
    dot_general x2, matrix products, swiglu_rows(): return jnp.dot(hidden, down_matrix, preferred_element_type=jnp.float32)  15.6 us
  transfers between devices with their start and end apart: 7, of which 7 were waited for; matrix products, arithmetic and copies ran while one was open for 11% of the time, Pallas kernels for 0%

profile of v1, /device:TPU:0, one launch (start us, length us, event | category | flops | bytes accessed | tf_op | source)
XLA Modules:
  0.0 507.0 jit_solution(15531483860759654351)
XLA Ops:
  13.5 7.4 %all-to-all-start.1 = ((bf16[16,3,48,1,512]{4,2,1,3,0:T(8,128)(2,1)}), bf16[16,3,48,1,512]{4,2,1,3,0:T(8,128)(2,1)S(1)}, u32[]{:S(2)}, u32[]{:S(2)}) async-start(bf16[16,3,48,1,512]{4,2,1,3,0:T(8,128)(2,1)} %pad_maximum_fusion), calls=%async_computation.1 | async-start | bytes 4718592 | tf_op jit(solution)/shard_map/all_to_all | solution.py:42
  21.2 4.5 reduce-window.6
  26.9 4.3 scatter_custom_fusion
  31.2 7.1 %gather_fusion = bf16[1536,2048]{1,0:T(8,128)(2,1)} fusion(bf16[129,2048]{1,0:T(8,128)(2,1)S(1)} %concatenate.11, s32[2048]{0:T(1024)S(1)} %pad_clamp_fusion), kind=kCustom, calls=%fused_computation | custom fusion | bytes 12589056 | tf_op jit(solution)/shard_map/gather | solution.py:93
  38.3 36.5 %all-to-all-done.1 = bf16[16,3,48,1,512]{4,2,1,3,0:T(8,128)(2,1)S(1)} async-done(((bf16[16,3,48,1,512]{4,2,1,3,0:T(8,128)(2,1)}), bf16[16,3,48,1,512]{4,2,1,3,0:T(8,128)(2,1)S(1)}, u32[]{:S(2)}, u32[]{:S(2)}) %all-to-all-start.1) | async-done | bytes 2359328 | tf_op jit(solution)/shard_map/all_to_all | solution.py:42
  75.4 6.5 %all_to_all.30 = bf16[2,1,3,384,1,512]{5,3,2,4,1,0:T(8,128)(2,1)} all-to-all(bf16[2,1,3,384,1,512]{5,3,2,4,1,0:T(8,128)(2,1)S(1)} %pad_maximum_fusion.1), channel_id=1, replica_groups=mesh['gr'=2,'fs'=8,'tp'=2] {'tp'}, dimensions={0} | all-to-all | bytes 4718592 | tf_op jit(solution)/shard_map/all_to_all | solution.py:39
  81.9 4.7 all-to-all-start
  87.3 65.5 %all-gather.9.cloned.1.call-done = bf16[1,3,384,4,1,512]{5,2,4,1,0,3:T(8,128)(2,1)} async-done(((bf16[1,3,384,2,1,512]{5,2,4,1,0,3:T(8,128)(2,1)}), bf16[1,3,384,4,1,512]{5,2,4,1,0,3:T(8,128)(2,1)}) %all-gather.9.cloned.1.call-update) | async-done | bytes 4718608 | tf_op jit(solution)/shard_map/all_gather | solution.py:55
  152.8 6.6 %copy.48 = bf16[1,3,384,4,1,512]{2,5,3,1,4,0:T(8,128)(2,1)} copy(bf16[1,3,384,4,1,512]{5,2,4,1,0,3:T(8,128)(2,1)} %all-gather.9.cloned.1.call-done) | data formatting | bytes 9437184 | tf_op jit(solution)/shard_map/all_gather | solution.py:55
  159.5 41.1 %all-to-all-done = bf16[16,96,2048]{2,1,0:T(8,128)(2,1)} async-done(((bf16[16,96,2048]{2,1,0:T(8,128)(2,1)}), bf16[16,96,2048]{2,1,0:T(8,128)(2,1)}, u32[]{:S(2)}, u32[]{:S(2)}) %all-to-all-start) | async-done | bytes 6291488 | tf_op jit(solution)/shard_map/all_to_all | solution.py:94
  200.6 5.9 %fusion.10 = f32[1536,384]{1,0:T(8,128)S(1)} fusion(bf16[1536,2048]{1,0:T(8,128)(2,1)} %bitcast.5, bf16[1,3,384,2048]{2,3,1,0:T(8,128)(2,1)} %bitcast.93), kind=kOutput, calls=%fused_computation.19 | convolution fusion | flops 2415919104 | bytes 10223616 | tf_op jit(solution)/shard_map/dot_general | solution.py:10
  206.5 11.4 %convolution_convert_fusion = bf16[1536,2048]{1,0:T(8,128)(2,1)} fusion(bf16[1,3,384,2048]{2,3,1,0:T(8,128)(2,1)} %bitcast.94, bf16[1536,2048]{1,0:T(8,128)(2,1)} %bitcast.5, f32[1536,384]{1,0:T(8,128)S(1)} %fusion.10), kind=kOutput, calls=%fused_computation.5 | convolution fusion | flops 4838522880 | bytes 18087936 | tf_op jit(solution)/shard_map/dot_general | solution.py:19
  217.9 28.2 %all-to-all-start.3 = ((bf16[16,96,2048]{2,1,0:T(8,128)(2,1)}), bf16[16,96,2048]{2,1,0:T(8,128)(2,1)}, u32[]{:S(2)}, u32[]{:S(2)}) async-start(bf16[16,96,2048]{2,1,0:T(8,128)(2,1)} %bitcast.98), calls=%async_computation.3 | async-start | bytes 12582912 | tf_op jit(solution)/shard_map/all_to_all | solution.py:100
  246.3 8.7 %all_gather.16 = bf16[3,64,2048]{2,1,0:T(8,128)(2,1)S(1)} all-gather(bf16[3,64,512]{2,1,0:T(8,128)(2,1)S(1)} %pad_maximum_fusion.2), channel_id=1, replica_groups=mesh['gr'=2,'fs'=8,'tp'=2] {'gr','tp'}, dimensions={2}, use_global_device_ids=true | all-gather | bytes 983040 | tf_op jit(solution)/shard_map/all_gather | solution.py:65
  257.6 111.5 %all-gather.11.cloned.1.call-done = bf16[1,512,2048]{2,1,0:T(8,128)(2,1)} async-done(((bf16[1,64,2048]{2,1,0:T(8,128)(2,1)}), bf16[1,512,2048]{2,1,0:T(8,128)(2,1)}) %all-gather.11.cloned.1.call-update) | async-done | bytes 2097168 | tf_op jit(solution)/shard_map/all_gather | solution.py:77
  371.5 4.5 slice_bitcast_fusion
  376.0 2.6 copy.50
  378.5 2.6 copy.51
  382.7 2.8 all-to-all-done.3
  385.5 12.4 %gather_fusion.1 = bf16[1024,2048]{1,0:T(8,128)(2,1)} fusion(bf16[1536,2048]{1,0:T(8,128)(2,1)} %bitcast.22, s32[1024]{0:T(1024)S(1)} %broadcast_clamp_fusion), kind=kCustom, calls=%fused_computation.1 | custom fusion | bytes 8392704 | tf_op jit(solution)/shard_map/gather | solution.py:101
  397.9 6.5 %fusion = f32[128,2048]{1,0:T(8,128)S(1)} fusion(bf16[1024,2048]{1,0:T(8,128)(2,1)} %gather_fusion.1, f32[128,8]{1,0:T(8,128)S(1)} %copy.49), kind=kLoop, calls=%fused_computation.4 | loop fusion | flops 6029312 | bytes 5246976 | tf_op jit(solution)/shard_map/reduce_sum | solution.py:103
  404.4 40.6 %all-gather.13.cloned.1.call-done = bf16[1,512,2048]{2,1,0:T(8,128)(2,1)} async-done(((bf16[1,64,2048]{2,1,0:T(8,128)(2,1)}), bf16[1,512,2048]{2,1,0:T(8,128)(2,1)}) %all-gather.13.cloned.1.call-update) | async-done | bytes 2097168 | tf_op jit(solution)/shard_map/all_gather | solution.py:78
  445.0 50.2 %all-gather.15.cloned.1.call-done = bf16[1,512,2048]{2,1,0:T(8,128)(2,1)} async-done(((bf16[1,64,2048]{2,1,0:T(8,128)(2,1)}), bf16[1,512,2048]{2,1,0:T(8,128)(2,1)}) %all-gather.15.cloned.1.call-update) | async-done | bytes 2097168 | tf_op jit(solution)/shard_map/all_gather | solution.py:79
  495.2 4.3 fusion.2
  (61 shorter events, 14.7 us)
Async XLA Ops:
  8.0 1.7 copy-start.6
  8.0 1.9 copy-start.1
  13.5 7.4 %copy-start.5 = (s32[128,8]{0,1:T(8,128)S(1)}, s32[128,8]{0,1:T(8,128)}, u32[]{:S(2)}) copy-start(s32[128,8]{0,1:T(8,128)} %param.11) | copy-start | bytes 12292
  13.5 12.8 %copy-start = (bf16[128,2048]{1,0:T(8,128)(2,1)S(1)}, bf16[128,2048]{1,0:T(8,128)(2,1)}, u32[]{:S(2)}) copy-start(bf16[128,2048]{1,0:T(8,128)(2,1)} %param.10) | copy-start | bytes 1572868
  13.5 61.3 %all-to-all-start.1 = ((bf16[16,3,48,1,512]{4,2,1,3,0:T(8,128)(2,1)}), bf16[16,3,48,1,512]{4,2,1,3,0:T(8,128)(2,1)S(1)}, u32[]{:S(2)}, u32[]{:S(2)}) async-start(bf16[16,3,48,1,512]{4,2,1,3,0:T(8,128)(2,1)} %pad_maximum_fusion), calls=%async_computation.1 | async-start | bytes 4718592 | tf_op jit(solution)/shard_map/all_to_all | solution.py:42
  81.9 118.7 %all-to-all-start = ((bf16[16,96,2048]{2,1,0:T(8,128)(2,1)}), bf16[16,96,2048]{2,1,0:T(8,128)(2,1)}, u32[]{:S(2)}, u32[]{:S(2)}) async-start(bf16[16,96,2048]{2,1,0:T(8,128)(2,1)} %bitcast.92), calls=%async_computation | async-start | bytes 12582912 | tf_op jit(solution)/shard_map/all_to_all | solution.py:94
  86.6 66.2 %all-gather.9.cloned.1.call-start = ((), (), s32[]{:S(2)}) async-start(), calls=%async_computation.4 | async-start | bytes 7077888 | tf_op jit(solution)/shard_map/all_gather | solution.py:55
  217.9 28.3 %copy-start.4 = (f32[64,512]{1,0:T(8,128)S(1)}, f32[64,512]{1,0:T(8,128)}, u32[]{:S(2)}) copy-start(f32[64,512]{1,0:T(8,128)} %param.19) | copy-start | bytes 393220
  217.9 28.3 %copy-start.2 = (f32[64,512]{1,0:T(8,128)S(1)}, f32[64,512]{1,0:T(8,128)}, u32[]{:S(2)}) copy-start(f32[64,512]{1,0:T(8,128)} %param.17) | copy-start | bytes 393220
  217.9 28.3 %copy-start.3 = (f32[64,512]{1,0:T(8,128)S(1)}, f32[64,512]{1,0:T(8,128)}, u32[]{:S(2)}) copy-start(f32[64,512]{1,0:T(8,128)} %param.18) | copy-start | bytes 393220
  217.9 167.6 %all-to-all-start.3 = ((bf16[16,96,2048]{2,1,0:T(8,128)(2,1)}), bf16[16,96,2048]{2,1,0:T(8,128)(2,1)}, u32[]{:S(2)}, u32[]{:S(2)}) async-start(bf16[16,96,2048]{2,1,0:T(8,128)(2,1)} %bitcast.98), calls=%async_computation.3 | async-start | bytes 12582912 | tf_op jit(solution)/shard_map/all_to_all | solution.py:100
  246.2 122.9 %all-gather.11.cloned.1.call-start = ((), (), s32[]{:S(2)}) async-start(), calls=%async_computation.5 | async-start | bytes 2359296 | tf_op jit(solution)/shard_map/all_gather | solution.py:77
  246.3 11.2 %copy-start.7 = (f32[128,8]{0,1:T(8,128)S(1)}, f32[128,8]{0,1:T(8,128)}, u32[]{:S(2)}) copy-start(f32[128,8]{0,1:T(8,128)} %param.12) | copy-start | bytes 12292
  256.3 188.7 %all-gather.13.cloned.1.call-start = ((), (), s32[]{:S(2)}) async-start(), calls=%async_computation.6 | async-start | bytes 2359296 | tf_op jit(solution)/shard_map/all_gather | solution.py:78
  256.9 238.3 %all-gather.15.cloned.1.call-start = ((), (), s32[]{:S(2)}) async-start(), calls=%async_computation.7 | async-start | bytes 2359296 | tf_op jit(solution)/shard_map/all_gather | solution.py:79
Sparse Core Ops, SparseCore 0:
  88.9 63.8 all-gather.8
Sparse Core Ops, SparseCore 1:
  256.4 112.6 all-gather.10
  371.0 73.9 all-gather.12
  447.6 47.5 all-gather.14
